TPU v7x, 32 devices: a whole 2x2x4 slice. The times are simulated.
32 devices in a mesh: ep: 8 (over z, x), tp: 4 (over y, core).
Axes of the slice: x: 2, y: 2, z: 4, core: 2. Of those that a mesh axis runs over, the one named last changes fastest.
Arguments:
- query_rows: bfloat16 [1024, 1024], P('ep', 'tp'), may hold values from -6 to 6
- key_rows: bfloat16 [1024, 256], P('ep', 'tp'), may hold values from -6 to 6
- retrieved_vector_table: bfloat16 [1024, 256], P('ep', 'tp'), may hold values from -6 to 6
- key_bias: bfloat16 [1024, 4], P('ep', 'tp'), may hold values from -1.5 to 12
- score_offset: float32 [16], P('tp'), may hold values from 3 to 12
- out_weight: bfloat16 [1024, 2048], P('tp'), may hold values from -0.1875 to 0.1875
- second_batch_activations: bfloat16 [1024, 2048], P('ep'), may hold values from -6 to 6
- norm_gain: float32 [2048], replicated, may hold values from 0.1 to 1.9
- expert_index: int32 [1024, 2], P('ep'), may hold values from 0 to 7, all different within a row; in each aligned block of 128 rows (0 to 127, 128 to 255, ...) at most 64 rows name the same one
- route_weight: float32 [1024, 2], P('ep'), may hold values from 0.2 to 1
- gate_weight: bfloat16 [8, 2048, 1024], P('ep', None, 'tp'), may hold values from -0.125 to 0.125
- up_weight: bfloat16 [8, 2048, 1024], P('ep', None, 'tp'), may hold values from -0.125 to 0.125
- down_weight: bfloat16 [8, 1024, 2048], P('ep', 'tp'), may hold values from -0.1875 to 0.1875
Outputs:
- attention_out: bfloat16 [1024, 2048], P(('ep', 'tp'))
- expert_out: bfloat16 [1024, 2048], P('ep', 'tp')
Inputs may be any that keep to these rules, and one draw needn't show every extreme that they name: `expert_index`: each row names 2 different experts; in each aligned block of 128 rows (the rows of one index of ep) no expert is named by more than 64 rows, a bound that some block reaches.
All inputs are finite; a program needn't handle non-finite values.
Results may differ from a plain program's by a relative error of at most 0.011.
Values may be sent and summed in bfloat16 or wider, within the bound.
A program may use at most 64 MiB of HBM per device.

v0:
```python
import math

import jax
import jax.numpy as jnp
from jax import lax
from jax.sharding import PartitionSpec as P

HD = 64
SEQS = 1


def passed_along(array, axis, by):
    peers = lax.axis_size(axis)
    pairs = [(i, i + by) for i in range(peers) if 0 <= i + by < peers]
    return lax.ppermute(array, axis, pairs)


def block_terms(query_block, key_block, value_block, bias_block, offset, causal_mask):
    scale = 1.0 / math.sqrt(query_block.shape[-1])
    scores = (
        jnp.einsum("tkgd,skd->kgts", query_block, key_block, preferred_element_type=jnp.float32)
        * scale
    )
    scores = (
        scores
        + jnp.transpose(bias_block.astype(jnp.float32))[:, None, None, :]
        - offset[:, :, None, None]
    )
    length = query_block.shape[0]
    if causal_mask:
        later = lax.broadcasted_iota(jnp.int32, (length, length), 0) > lax.broadcasted_iota(
            jnp.int32, (length, length), 1
        )
        keep = jnp.where(later, jax.nn.log_sigmoid(-scores), 0.0)
        suffix = lax.cumsum(keep, axis=3, reverse=True) - keep
        weight = jnp.where(later, jnp.exp(jax.nn.log_sigmoid(scores) + suffix), 0.0)
    else:
        keep = jax.nn.log_sigmoid(-scores)
        suffix = lax.cumsum(keep, axis=3, reverse=True) - keep
        weight = jnp.exp(jax.nn.log_sigmoid(scores) + suffix)
    weight = weight.astype(jnp.bfloat16)
    block_out = jnp.einsum(
        "kgts,skd->kgtd", weight, value_block, preferred_element_type=jnp.float32
    )
    return (block_out, jnp.sum(keep, axis=3))


def attention_half(
    query_rows, key_rows, retrieved_vector_table, key_bias, score_offset, out_weight
):
    length = query_rows.shape[0]
    kv_local = key_rows.shape[1] // HD
    group = query_rows.shape[1] // HD // kv_local
    query_block = query_rows.reshape(length, kv_local, group, HD)
    key_block = key_rows.reshape(length, kv_local, HD)
    value_block = retrieved_vector_table.reshape(length, kv_local, HD)
    offset = score_offset.reshape(kv_local, group)
    span = lax.axis_size("ep") // SEQS
    sequence_place_index = lax.axis_index("ep") % span
    result, near = block_terms(query_block, key_block, value_block, key_bias, offset, True)

    def step(distance, state):
        result, near, moving = state
        moving = passed_along((moving[0], moving[1], moving[2]), "ep", 1)
        block_out, total = block_terms(query_block, moving[0], moving[1], moving[2], offset, False)
        valid = sequence_place_index >= distance
        result = jnp.where(valid, result + jnp.exp(near)[..., None] * block_out, result)
        near = jnp.where(valid, near + total, near)
        return (result, near, moving)

    result, near, moving = lax.fori_loop(
        1, span, step, (result, near, (key_block, value_block, key_bias))
    )
    attended = (
        jnp.transpose(result, (2, 0, 1, 3))
        .reshape(length, kv_local * group * HD)
        .astype(jnp.bfloat16)
    )
    return lax.psum_scatter(
        jnp.dot(attended, out_weight, preferred_element_type=jnp.float32).astype(jnp.bfloat16),
        "tp",
        scatter_dimension=0,
        tiled=True,
    )


def expert_half(
    second_batch_activations,
    norm_gain,
    expert_index,
    route_weight,
    gate_weight,
    up_weight,
    down_weight,
):
    tokens = second_batch_activations.shape[0]
    picks = expert_index.shape[1]
    experts = lax.axis_size("ep")
    capacity = 2 * tokens * picks // experts
    values32 = second_batch_activations.astype(jnp.float32)
    normed = (
        values32
        * lax.rsqrt(jnp.mean(values32 * values32, axis=1, keepdims=True) + 1e-06)
        * norm_gain
    ).astype(jnp.bfloat16)
    flat = expert_index.reshape(-1)
    indicator_matrix = (flat[:, None] == jnp.arange(experts, dtype=jnp.int32)[None, :]).astype(
        jnp.int32
    )
    slot = jnp.sum(indicator_matrix * (jnp.cumsum(indicator_matrix, axis=0) - 1), axis=1)
    target = flat * capacity + slot
    source_row = (
        jnp.full((experts * capacity,), tokens, jnp.int32)
        .at[target]
        .set(jnp.arange(flat.shape[0], dtype=jnp.int32) // picks)
    )
    padded = jnp.concatenate([normed, jnp.zeros((1, normed.shape[1]), jnp.bfloat16)], axis=0)
    quarter = padded.shape[1] // lax.axis_size("tp")
    columns = lax.dynamic_slice_in_dim(padded, lax.axis_index("tp") * quarter, quarter, 1)
    outgoing = columns[source_row].reshape(experts, capacity, quarter)
    gate_local = gate_weight[0]
    up_local = up_weight[0]
    down_local = down_weight[0]
    piece = lax.all_gather(
        lax.all_to_all(outgoing, "ep", split_axis=0, concat_axis=0, tiled=True),
        "tp",
        axis=2,
        tiled=True,
    )
    gate_pre = jnp.einsum("scd,df->scf", piece, gate_local, preferred_element_type=jnp.float32)
    up_pre = jnp.einsum("scd,df->scf", piece, up_local, preferred_element_type=jnp.float32)
    hidden = (jax.nn.silu(gate_pre) * up_pre).astype(jnp.bfloat16)
    partial_value = jnp.einsum(
        "scf,fd->scd", hidden, down_local, preferred_element_type=jnp.float32
    )
    summed = lax.psum_scatter(
        partial_value.astype(jnp.bfloat16), "tp", scatter_dimension=2, tiled=True
    )
    returned = lax.all_to_all(summed, "ep", split_axis=0, concat_axis=0, tiled=True)
    picked = returned.reshape(experts * capacity, returned.shape[2])[target].reshape(
        tokens, picks, returned.shape[2]
    )
    return jnp.sum(route_weight[:, :, None] * picked.astype(jnp.float32), axis=1).astype(
        jnp.bfloat16
    )


def body(
    query_rows,
    key_rows,
    retrieved_vector_table,
    key_bias,
    score_offset,
    out_weight,
    second_batch_activations,
    norm_gain,
    expert_index,
    route_weight,
    gate_weight,
    up_weight,
    down_weight,
):
    attention_out = attention_half(
        query_rows, key_rows, retrieved_vector_table, key_bias, score_offset, out_weight
    )
    expert_out = expert_half(
        second_batch_activations,
        norm_gain,
        expert_index,
        route_weight,
        gate_weight,
        up_weight,
        down_weight,
    )
    return (attention_out, expert_out)


def solution(mesh):
    return jax.shard_map(
        body,
        mesh=mesh,
        in_specs=(
            P("ep", "tp"),
            P("ep", "tp"),
            P("ep", "tp"),
            P("ep", "tp"),
            P("tp"),
            P("tp", None),
            P("ep", None),
            P(),
            P("ep", None),
            P("ep", None),
            P("ep", None, "tp"),
            P("ep", None, "tp"),
            P("ep", "tp", None),
        ),
        out_specs=(P(("ep", "tp"), None), P("ep", "tp")),
        check_vma=False,
    )
```

profile of v0, /device:TPU:0, one launch (start us, length us, event | category | flops | bytes accessed | tf_op | source)
XLA Modules:
  0.0 208.5 jit_solution(2058096488093113496)
XLA Ops:
  18.3 21.7 %all_to_all.10 = bf16[8,64,512]{2,1,0:T(8,128)(2,1)} all-to-all(bf16[8,64,512]{2,1,0:T(8,128)(2,1)S(1)} %bitcast.118), channel_id=1, replica_groups=mesh['ep'=8,'tp'=4] {'ep'}, dimensions={0} | all-to-all | bytes 1048576 | tf_op jit(solution)/shard_map/all_to_all | solution.py:125
  40.7 4.4 %reduce_window_sum.33 = f32[1,4,128,128]{2,3,1,0:T(8,128)S(1)} reduce-window(f32[1,4,128,128]{2,3,1,0:T(8,128)S(1)} %get-tuple-element.181, f32[]{:T(128)} %constant.86.clone.1), window={size=1x1x1x128 pad=0_0x0_0x0_0x0_127}, to_apply=%region_0.1 | reduce-window | flops 8323072 | bytes 524292 | tf_op jit(solution)/shard_map/block_terms/reduce_window_sum | solution.py:35
  45.6 16.2 %all-gather.2.cloned.1.call-done = bf16[8,64,2048]{2,1,0:T(8,128)(2,1)} async-done(((bf16[8,64,512]{2,1,0:T(8,128)(2,1)}), bf16[8,64,2048]{2,1,0:T(8,128)(2,1)}) %all-gather.2.cloned.1.call-update) | async-done | bytes 2097168 | tf_op jit(solution)/shard_map/all_gather | solution.py:124
  61.8 3.5 %fusion.31 = f32[8,64,256]{2,1,0:T(8,128)} fusion(bf16[8,64,2048]{2,1,0:T(8,128)(2,1)} %all-gather.2.cloned.1.call-done, bf16[1,2048,256]{2,1,0:T(8,128)(2,1)} %param.25), kind=kOutput, calls=%fused_computation.45 | convolution fusion | flops 536870912 | bytes 3670016 | tf_op jit(solution)/shard_map/scd,df->scf/dot_general | solution.py:130
  65.3 5.0 %convolution_convert_fusion = bf16[8,64,2048]{2,1,0:T(8,128)(2,1)} fusion(bf16[8,64,2048]{2,1,0:T(8,128)(2,1)S(1)} %copy-done.4, bf16[1,256,2048]{2,1,0:T(8,128)(2,1)S(1)} %copy-done, bf16[1,2048,256]{2,1,0:T(8,128)(2,1)} %param.26, f32[8,64,256]{2,1,0:T(8,128)} %fusion.31), kind=kOutput, calls=%fused_computation.28 | convolution fusion | flops 1075576832 | bytes 6815744 | tf_op jit(solution)/shard_map/scf,fd->scd/dot_general | solution.py:133
  70.4 102.1 %while.21 = (s32[]{:T(128)}, f32[1,4,128,64]{2,3,1,0:T(8,128)S(1)}, f32[1,4,128]{2,1,0:T(4,128)S(1)}, bf16[128,1,64]{0,2,1:T(8,128)(2,1)S(1)}, bf16[128,1,64]{0,...) while((s32[]{:T(128)}, f32[1,4,128,64]{2,3,1,0:T(8,128)S(1)}, ...), condition=%wide.region_5.6_spmd, body=%wide.region_2.5_spmd.sunk | while | flops 27100288 | bytes 2145284 | solution.py:71
  70.6 3.5 %collective-permute-start.1 = (bf16[128,1,64]{0,2,1:T(8,128)(2,1)S(1)}, bf16[128,1,64]{0,2,1:T(8,128)(2,1)S(1)}, u32[]{:S(2)}, u32[]{:S(2)}) collective-permute-start(bf16[128,1,64]{0,2,1:T(8,128)(2,1)S(1)} %get-tuple-element.262), channel_id=1, source_target_pairs={{0,4},{4,8},{8,12},{12,16},{16,20},{20,24},{24,28},{1,5},{5,9},{9,... | collective-permute-start | bytes 49160 | tf_op jit(solution)/shard_map/while/body/eval_jaxpr/ppermute | solution.py:15
  74.1 3.4 %collective-permute-start = (bf16[128,1]{0,1:T(2,128)(2,1)S(1)}, bf16[128,1]{0,1:T(2,128)(2,1)S(1)}, u32[]{:S(2)}, u32[]{:S(2)}) collective-permute-start(bf16[128,1]{0,1:T(2,128)(2,1)S(1)} %get-tuple-element.264), channel_id=1, source_target_pairs={{0,4},{4,8},{8,12},{12,16},{16,20},{20,24},{24,28},{1,5},{5,9},{9,... | collective-permute-start | bytes 776 | tf_op jit(solution)/shard_map/while/body/eval_jaxpr/ppermute | solution.py:15
  81.3 4.4 %reduce_window_sum.37 = f32[1,4,128,128]{2,3,1,0:T(8,128)S(1)} reduce-window(f32[1,4,128,128]{2,3,1,0:T(8,128)S(1)} %get-tuple-element.243, f32[]{:T(128)} %constant.86.clone.1..sunk), window={size=1x1x1x128 pad=0_0x0_0x0_0x0_127}, to_apply=%region_3.3 | reduce-window | flops 8323072 | bytes 524292 | tf_op jit(solution)/shard_map/while/body/eval_jaxpr/reduce_window_sum | solution.py:35
  86.3 3.4 %collective-permute-start.1 = (bf16[128,1,64]{0,2,1:T(8,128)(2,1)S(1)}, bf16[128,1,64]{0,2,1:T(8,128)(2,1)S(1)}, u32[]{:S(2)}, u32[]{:S(2)}) collective-permute-start(bf16[128,1,64]{0,2,1:T(8,128)(2,1)S(1)} %get-tuple-element.262), channel_id=1, source_target_pairs={{0,4},{4,8},{8,12},{12,16},{16,20},{20,24},{24,28},{1,5},{5,9},{9,... | collective-permute-start | bytes 49160 | tf_op jit(solution)/shard_map/while/body/eval_jaxpr/ppermute | solution.py:15
  93.1 3.4 %collective-permute-start.2 = (bf16[128,1,64]{0,2,1:T(8,128)(2,1)S(1)}, bf16[128,1,64]{0,2,1:T(8,128)(2,1)S(1)}, u32[]{:S(2)}, u32[]{:S(2)}) collective-permute-start(bf16[128,1,64]{0,2,1:T(8,128)(2,1)S(1)} %get-tuple-element.263), channel_id=1, source_target_pairs={{0,4},{4,8},{8,12},{12,16},{16,20},{20,24},{24,28},{1,5},{5,9},{9,... | collective-permute-start | bytes 49160 | tf_op jit(solution)/shard_map/while/body/eval_jaxpr/ppermute | solution.py:15
  96.9 4.4 %reduce_window_sum.37 = f32[1,4,128,128]{2,3,1,0:T(8,128)S(1)} reduce-window(f32[1,4,128,128]{2,3,1,0:T(8,128)S(1)} %get-tuple-element.243, f32[]{:T(128)} %constant.86.clone.1..sunk), window={size=1x1x1x128 pad=0_0x0_0x0_0x0_127}, to_apply=%region_3.3 | reduce-window | flops 8323072 | bytes 524292 | tf_op jit(solution)/shard_map/while/body/eval_jaxpr/reduce_window_sum | solution.py:35
  112.0 4.4 %reduce_window_sum.37 = f32[1,4,128,128]{2,3,1,0:T(8,128)S(1)} reduce-window(f32[1,4,128,128]{2,3,1,0:T(8,128)S(1)} %get-tuple-element.243, f32[]{:T(128)} %constant.86.clone.1..sunk), window={size=1x1x1x128 pad=0_0x0_0x0_0x0_127}, to_apply=%region_3.3 | reduce-window | flops 8323072 | bytes 524292 | tf_op jit(solution)/shard_map/while/body/eval_jaxpr/reduce_window_sum | solution.py:35
  119.1 4.3 %collective-permute-start = (bf16[128,1]{0,1:T(2,128)(2,1)S(1)}, bf16[128,1]{0,1:T(2,128)(2,1)S(1)}, u32[]{:S(2)}, u32[]{:S(2)}) collective-permute-start(bf16[128,1]{0,1:T(2,128)(2,1)S(1)} %get-tuple-element.264), channel_id=1, source_target_pairs={{0,4},{4,8},{8,12},{12,16},{16,20},{20,24},{24,28},{1,5},{5,9},{9,... | collective-permute-start | bytes 776 | tf_op jit(solution)/shard_map/while/body/eval_jaxpr/ppermute | solution.py:15
  125.7 4.4 %reduce_window_sum.37 = f32[1,4,128,128]{2,3,1,0:T(8,128)S(1)} reduce-window(f32[1,4,128,128]{2,3,1,0:T(8,128)S(1)} %get-tuple-element.243, f32[]{:T(128)} %constant.86.clone.1..sunk), window={size=1x1x1x128 pad=0_0x0_0x0_0x0_127}, to_apply=%region_3.3 | reduce-window | flops 8323072 | bytes 524292 | tf_op jit(solution)/shard_map/while/body/eval_jaxpr/reduce_window_sum | solution.py:35
  130.7 3.5 %collective-permute-start.1 = (bf16[128,1,64]{0,2,1:T(8,128)(2,1)S(1)}, bf16[128,1,64]{0,2,1:T(8,128)(2,1)S(1)}, u32[]{:S(2)}, u32[]{:S(2)}) collective-permute-start(bf16[128,1,64]{0,2,1:T(8,128)(2,1)S(1)} %get-tuple-element.262), channel_id=1, source_target_pairs={{0,4},{4,8},{8,12},{12,16},{16,20},{20,24},{24,28},{1,5},{5,9},{9,... | collective-permute-start | bytes 49160 | tf_op jit(solution)/shard_map/while/body/eval_jaxpr/ppermute | solution.py:15
  140.1 4.4 %reduce_window_sum.37 = f32[1,4,128,128]{2,3,1,0:T(8,128)S(1)} reduce-window(f32[1,4,128,128]{2,3,1,0:T(8,128)S(1)} %get-tuple-element.243, f32[]{:T(128)} %constant.86.clone.1..sunk), window={size=1x1x1x128 pad=0_0x0_0x0_0x0_127}, to_apply=%region_3.3 | reduce-window | flops 8323072 | bytes 524292 | tf_op jit(solution)/shard_map/while/body/eval_jaxpr/reduce_window_sum | solution.py:35
  147.9 3.5 %collective-permute-start = (bf16[128,1]{0,1:T(2,128)(2,1)S(1)}, bf16[128,1]{0,1:T(2,128)(2,1)S(1)}, u32[]{:S(2)}, u32[]{:S(2)}) collective-permute-start(bf16[128,1]{0,1:T(2,128)(2,1)S(1)} %get-tuple-element.264), channel_id=1, source_target_pairs={{0,4},{4,8},{8,12},{12,16},{16,20},{20,24},{24,28},{1,5},{5,9},{9,... | collective-permute-start | bytes 776 | tf_op jit(solution)/shard_map/while/body/eval_jaxpr/ppermute | solution.py:15
  153.8 4.4 %reduce_window_sum.37 = f32[1,4,128,128]{2,3,1,0:T(8,128)S(1)} reduce-window(f32[1,4,128,128]{2,3,1,0:T(8,128)S(1)} %get-tuple-element.243, f32[]{:T(128)} %constant.86.clone.1..sunk), window={size=1x1x1x128 pad=0_0x0_0x0_0x0_127}, to_apply=%region_3.3 | reduce-window | flops 8323072 | bytes 524292 | tf_op jit(solution)/shard_map/while/body/eval_jaxpr/reduce_window_sum | solution.py:35
  158.8 3.5 %collective-permute-start.1 = (bf16[128,1,64]{0,2,1:T(8,128)(2,1)S(1)}, bf16[128,1,64]{0,2,1:T(8,128)(2,1)S(1)}, u32[]{:S(2)}, u32[]{:S(2)}) collective-permute-start(bf16[128,1,64]{0,2,1:T(8,128)(2,1)S(1)} %get-tuple-element.262), channel_id=1, source_target_pairs={{0,4},{4,8},{8,12},{12,16},{16,20},{20,24},{24,28},{1,5},{5,9},{9,... | collective-permute-start | bytes 49160 | tf_op jit(solution)/shard_map/while/body/eval_jaxpr/ppermute | solution.py:15
  167.5 4.4 %reduce_window_sum.37 = f32[1,4,128,128]{2,3,1,0:T(8,128)S(1)} reduce-window(f32[1,4,128,128]{2,3,1,0:T(8,128)S(1)} %get-tuple-element.243, f32[]{:T(128)} %constant.86.clone.1..sunk), window={size=1x1x1x128 pad=0_0x0_0x0_0x0_127}, to_apply=%region_3.3 | reduce-window | flops 8323072 | bytes 524292 | tf_op jit(solution)/shard_map/while/body/eval_jaxpr/reduce_window_sum | solution.py:35
  172.5 3.5 %all-to-all-start.1 = ((bf16[8,64,512]{2,1,0:T(8,128)(2,1)}), bf16[8,64,512]{2,1,0:T(8,128)(2,1)S(1)}, u32[]{:S(2)}, u32[]{:S(2)}) async-start(bf16[8,64,512]{2,1,0:T(8,128)(2,1)} %reduce-scatter.5.cloned.1.call-done), calls=%async_computation.3 | async-start | bytes 1048576 | tf_op jit(solution)/shard_map/all_to_all | solution.py:139
  177.3 8.9 %all-to-all-done.1 = bf16[8,64,512]{2,1,0:T(8,128)(2,1)S(1)} async-done(((bf16[8,64,512]{2,1,0:T(8,128)(2,1)}), bf16[8,64,512]{2,1,0:T(8,128)(2,1)S(1)}, u32[]{:S(2)}, u32[]{:S(2)}) %all-to-all-start.1) | async-done | bytes 524320 | tf_op jit(solution)/shard_map/all_to_all | solution.py:139
  189.1 12.9 %reduce-scatter.3.cloned.1.call-done = bf16[32,2048]{1,0:T(8,128)(2,1)} async-done(((bf16[128,2048]{1,0:T(8,128)(2,1)}), bf16[32,2048]{1,0:T(8,128)(2,1)}) %reduce-scatter.3.cloned.1.call-update) | async-done | bytes 131088 | tf_op jit(solution)/shard_map/reduce_scatter | solution.py:79
  (139 shorter events, 58.0 us)
Async XLA Ops:
  7.2 54.6 %all-gather.2.cloned.1.call-start = ((), (), s32[]{:S(2)}) async-start(), calls=%async_computation.5 | async-start | bytes 2621440 | tf_op jit(solution)/shard_map/all_gather | solution.py:124
  40.0 132.4 %reduce-scatter.5.cloned.1.call-start = ((), (), s32[]{:S(2)}) async-start(), calls=%async_computation.6 | async-start | bytes 2621440 | tf_op jit(solution)/shard_map/reduce_scatter | solution.py:136
  70.6 10.3 %collective-permute-start.1 = (bf16[128,1,64]{0,2,1:T(8,128)(2,1)S(1)}, bf16[128,1,64]{0,2,1:T(8,128)(2,1)S(1)}, u32[]{:S(2)}, u32[]{:S(2)}) collective-permute-start(bf16[128,1,64]{0,2,1:T(8,128)(2,1)S(1)} %get-tuple-element.262), channel_id=1, source_target_pairs={{0,4},{4,8},{8,12},{12,16},{16,20},{20,24},{24,28},{1,5},{5,9},{9,... | collective-permute-start | bytes 49160 | tf_op jit(solution)/shard_map/while/body/eval_jaxpr/ppermute | solution.py:15
  74.1 6.8 %collective-permute-start = (bf16[128,1]{0,1:T(2,128)(2,1)S(1)}, bf16[128,1]{0,1:T(2,128)(2,1)S(1)}, u32[]{:S(2)}, u32[]{:S(2)}) collective-permute-start(bf16[128,1]{0,1:T(2,128)(2,1)S(1)} %get-tuple-element.264), channel_id=1, source_target_pairs={{0,4},{4,8},{8,12},{12,16},{16,20},{20,24},{24,28},{1,5},{5,9},{9,... | collective-permute-start | bytes 776 | tf_op jit(solution)/shard_map/while/body/eval_jaxpr/ppermute | solution.py:15
  77.5 8.3 %collective-permute-start.2 = (bf16[128,1,64]{0,2,1:T(8,128)(2,1)S(1)}, bf16[128,1,64]{0,2,1:T(8,128)(2,1)S(1)}, u32[]{:S(2)}, u32[]{:S(2)}) collective-permute-start(bf16[128,1,64]{0,2,1:T(8,128)(2,1)S(1)} %get-tuple-element.263), channel_id=1, source_target_pairs={{0,4},{4,8},{8,12},{12,16},{16,20},{20,24},{24,28},{1,5},{5,9},{9,... | collective-permute-start | bytes 49160 | tf_op jit(solution)/shard_map/while/body/eval_jaxpr/ppermute | solution.py:15
  86.3 10.2 %collective-permute-start.1 = (bf16[128,1,64]{0,2,1:T(8,128)(2,1)S(1)}, bf16[128,1,64]{0,2,1:T(8,128)(2,1)S(1)}, u32[]{:S(2)}, u32[]{:S(2)}) collective-permute-start(bf16[128,1,64]{0,2,1:T(8,128)(2,1)S(1)} %get-tuple-element.262), channel_id=1, source_target_pairs={{0,4},{4,8},{8,12},{12,16},{16,20},{20,24},{24,28},{1,5},{5,9},{9,... | collective-permute-start | bytes 49160 | tf_op jit(solution)/shard_map/while/body/eval_jaxpr/ppermute | solution.py:15
  89.7 6.8 %collective-permute-start = (bf16[128,1]{0,1:T(2,128)(2,1)S(1)}, bf16[128,1]{0,1:T(2,128)(2,1)S(1)}, u32[]{:S(2)}, u32[]{:S(2)}) collective-permute-start(bf16[128,1]{0,1:T(2,128)(2,1)S(1)} %get-tuple-element.264), channel_id=1, source_target_pairs={{0,4},{4,8},{8,12},{12,16},{16,20},{20,24},{24,28},{1,5},{5,9},{9,... | collective-permute-start | bytes 776 | tf_op jit(solution)/shard_map/while/body/eval_jaxpr/ppermute | solution.py:15
  93.1 8.3 %collective-permute-start.2 = (bf16[128,1,64]{0,2,1:T(8,128)(2,1)S(1)}, bf16[128,1,64]{0,2,1:T(8,128)(2,1)S(1)}, u32[]{:S(2)}, u32[]{:S(2)}) collective-permute-start(bf16[128,1,64]{0,2,1:T(8,128)(2,1)S(1)} %get-tuple-element.263), channel_id=1, source_target_pairs={{0,4},{4,8},{8,12},{12,16},{16,20},{20,24},{24,28},{1,5},{5,9},{9,... | collective-permute-start | bytes 49160 | tf_op jit(solution)/shard_map/while/body/eval_jaxpr/ppermute | solution.py:15
  101.9 9.7 %collective-permute-start.1 = (bf16[128,1,64]{0,2,1:T(8,128)(2,1)S(1)}, bf16[128,1,64]{0,2,1:T(8,128)(2,1)S(1)}, u32[]{:S(2)}, u32[]{:S(2)}) collective-permute-start(bf16[128,1,64]{0,2,1:T(8,128)(2,1)S(1)} %get-tuple-element.262), channel_id=1, source_target_pairs={{0,4},{4,8},{8,12},{12,16},{16,20},{20,24},{24,28},{1,5},{5,9},{9,... | collective-permute-start | bytes 49160 | tf_op jit(solution)/shard_map/while/body/eval_jaxpr/ppermute | solution.py:15
  105.3 6.3 %collective-permute-start = (bf16[128,1]{0,1:T(2,128)(2,1)S(1)}, bf16[128,1]{0,1:T(2,128)(2,1)S(1)}, u32[]{:S(2)}, u32[]{:S(2)}) collective-permute-start(bf16[128,1]{0,1:T(2,128)(2,1)S(1)} %get-tuple-element.264), channel_id=1, source_target_pairs={{0,4},{4,8},{8,12},{12,16},{16,20},{20,24},{24,28},{1,5},{5,9},{9,... | collective-permute-start | bytes 776 | tf_op jit(solution)/shard_map/while/body/eval_jaxpr/ppermute | solution.py:15
  108.2 8.3 %collective-permute-start.2 = (bf16[128,1,64]{0,2,1:T(8,128)(2,1)S(1)}, bf16[128,1,64]{0,2,1:T(8,128)(2,1)S(1)}, u32[]{:S(2)}, u32[]{:S(2)}) collective-permute-start(bf16[128,1,64]{0,2,1:T(8,128)(2,1)S(1)} %get-tuple-element.263), channel_id=1, source_target_pairs={{0,4},{4,8},{8,12},{12,16},{16,20},{20,24},{24,28},{1,5},{5,9},{9,... | collective-permute-start | bytes 49160 | tf_op jit(solution)/shard_map/while/body/eval_jaxpr/ppermute | solution.py:15
  117.0 8.3 %collective-permute-start.1 = (bf16[128,1,64]{0,2,1:T(8,128)(2,1)S(1)}, bf16[128,1,64]{0,2,1:T(8,128)(2,1)S(1)}, u32[]{:S(2)}, u32[]{:S(2)}) collective-permute-start(bf16[128,1,64]{0,2,1:T(8,128)(2,1)S(1)} %get-tuple-element.262), channel_id=1, source_target_pairs={{0,4},{4,8},{8,12},{12,16},{16,20},{20,24},{24,28},{1,5},{5,9},{9,... | collective-permute-start | bytes 49160 | tf_op jit(solution)/shard_map/while/body/eval_jaxpr/ppermute | solution.py:15
  119.1 6.2 %collective-permute-start = (bf16[128,1]{0,1:T(2,128)(2,1)S(1)}, bf16[128,1]{0,1:T(2,128)(2,1)S(1)}, u32[]{:S(2)}, u32[]{:S(2)}) collective-permute-start(bf16[128,1]{0,1:T(2,128)(2,1)S(1)} %get-tuple-element.264), channel_id=1, source_target_pairs={{0,4},{4,8},{8,12},{12,16},{16,20},{20,24},{24,28},{1,5},{5,9},{9,... | collective-permute-start | bytes 776 | tf_op jit(solution)/shard_map/while/body/eval_jaxpr/ppermute | solution.py:15
  123.3 6.8 %collective-permute-start.2 = (bf16[128,1,64]{0,2,1:T(8,128)(2,1)S(1)}, bf16[128,1,64]{0,2,1:T(8,128)(2,1)S(1)}, u32[]{:S(2)}, u32[]{:S(2)}) collective-permute-start(bf16[128,1,64]{0,2,1:T(8,128)(2,1)S(1)} %get-tuple-element.263), channel_id=1, source_target_pairs={{0,4},{4,8},{8,12},{12,16},{16,20},{20,24},{24,28},{1,5},{5,9},{9,... | collective-permute-start | bytes 49160 | tf_op jit(solution)/shard_map/while/body/eval_jaxpr/ppermute | solution.py:15
  130.7 9.0 %collective-permute-start.1 = (bf16[128,1,64]{0,2,1:T(8,128)(2,1)S(1)}, bf16[128,1,64]{0,2,1:T(8,128)(2,1)S(1)}, u32[]{:S(2)}, u32[]{:S(2)}) collective-permute-start(bf16[128,1,64]{0,2,1:T(8,128)(2,1)S(1)} %get-tuple-element.262), channel_id=1, source_target_pairs={{0,4},{4,8},{8,12},{12,16},{16,20},{20,24},{24,28},{1,5},{5,9},{9,... | collective-permute-start | bytes 49160 | tf_op jit(solution)/shard_map/while/body/eval_jaxpr/ppermute | solution.py:15
  134.2 5.4 %collective-permute-start = (bf16[128,1]{0,1:T(2,128)(2,1)S(1)}, bf16[128,1]{0,1:T(2,128)(2,1)S(1)}, u32[]{:S(2)}, u32[]{:S(2)}) collective-permute-start(bf16[128,1]{0,1:T(2,128)(2,1)S(1)} %get-tuple-element.264), channel_id=1, source_target_pairs={{0,4},{4,8},{8,12},{12,16},{16,20},{20,24},{24,28},{1,5},{5,9},{9,... | collective-permute-start | bytes 776 | tf_op jit(solution)/shard_map/while/body/eval_jaxpr/ppermute | solution.py:15
  137.0 7.5 %collective-permute-start.2 = (bf16[128,1,64]{0,2,1:T(8,128)(2,1)S(1)}, bf16[128,1,64]{0,2,1:T(8,128)(2,1)S(1)}, u32[]{:S(2)}, u32[]{:S(2)}) collective-permute-start(bf16[128,1,64]{0,2,1:T(8,128)(2,1)S(1)} %get-tuple-element.263), channel_id=1, source_target_pairs={{0,4},{4,8},{8,12},{12,16},{16,20},{20,24},{24,28},{1,5},{5,9},{9,... | collective-permute-start | bytes 49160 | tf_op jit(solution)/shard_map/while/body/eval_jaxpr/ppermute | solution.py:15
  145.1 8.3 %collective-permute-start.1 = (bf16[128,1,64]{0,2,1:T(8,128)(2,1)S(1)}, bf16[128,1,64]{0,2,1:T(8,128)(2,1)S(1)}, u32[]{:S(2)}, u32[]{:S(2)}) collective-permute-start(bf16[128,1,64]{0,2,1:T(8,128)(2,1)S(1)} %get-tuple-element.262), channel_id=1, source_target_pairs={{0,4},{4,8},{8,12},{12,16},{16,20},{20,24},{24,28},{1,5},{5,9},{9,... | collective-permute-start | bytes 49160 | tf_op jit(solution)/shard_map/while/body/eval_jaxpr/ppermute | solution.py:15
  147.9 5.4 %collective-permute-start = (bf16[128,1]{0,1:T(2,128)(2,1)S(1)}, bf16[128,1]{0,1:T(2,128)(2,1)S(1)}, u32[]{:S(2)}, u32[]{:S(2)}) collective-permute-start(bf16[128,1]{0,1:T(2,128)(2,1)S(1)} %get-tuple-element.264), channel_id=1, source_target_pairs={{0,4},{4,8},{8,12},{12,16},{16,20},{20,24},{24,28},{1,5},{5,9},{9,... | collective-permute-start | bytes 776 | tf_op jit(solution)/shard_map/while/body/eval_jaxpr/ppermute | solution.py:15
  151.4 6.8 %collective-permute-start.2 = (bf16[128,1,64]{0,2,1:T(8,128)(2,1)S(1)}, bf16[128,1,64]{0,2,1:T(8,128)(2,1)S(1)}, u32[]{:S(2)}, u32[]{:S(2)}) collective-permute-start(bf16[128,1,64]{0,2,1:T(8,128)(2,1)S(1)} %get-tuple-element.263), channel_id=1, source_target_pairs={{0,4},{4,8},{8,12},{12,16},{16,20},{20,24},{24,28},{1,5},{5,9},{9,... | collective-permute-start | bytes 49160 | tf_op jit(solution)/shard_map/while/body/eval_jaxpr/ppermute | solution.py:15
  158.8 8.3 %collective-permute-start.1 = (bf16[128,1,64]{0,2,1:T(8,128)(2,1)S(1)}, bf16[128,1,64]{0,2,1:T(8,128)(2,1)S(1)}, u32[]{:S(2)}, u32[]{:S(2)}) collective-permute-start(bf16[128,1,64]{0,2,1:T(8,128)(2,1)S(1)} %get-tuple-element.262), channel_id=1, source_target_pairs={{0,4},{4,8},{8,12},{12,16},{16,20},{20,24},{24,28},{1,5},{5,9},{9,... | collective-permute-start | bytes 49160 | tf_op jit(solution)/shard_map/while/body/eval_jaxpr/ppermute | solution.py:15
  165.1 6.8 %collective-permute-start.2 = (bf16[128,1,64]{0,2,1:T(8,128)(2,1)S(1)}, bf16[128,1,64]{0,2,1:T(8,128)(2,1)S(1)}, u32[]{:S(2)}, u32[]{:S(2)}) collective-permute-start(bf16[128,1,64]{0,2,1:T(8,128)(2,1)S(1)} %get-tuple-element.263), channel_id=1, source_target_pairs={{0,4},{4,8},{8,12},{12,16},{16,20},{20,24},{24,28},{1,5},{5,9},{9,... | collective-permute-start | bytes 49160 | tf_op jit(solution)/shard_map/while/body/eval_jaxpr/ppermute | solution.py:15
  172.5 13.7 %all-to-all-start.1 = ((bf16[8,64,512]{2,1,0:T(8,128)(2,1)}), bf16[8,64,512]{2,1,0:T(8,128)(2,1)S(1)}, u32[]{:S(2)}, u32[]{:S(2)}) async-start(bf16[8,64,512]{2,1,0:T(8,128)(2,1)} %reduce-scatter.5.cloned.1.call-done), calls=%async_computation.3 | async-start | bytes 1048576 | tf_op jit(solution)/shard_map/all_to_all | solution.py:139
  176.0 26.0 %reduce-scatter.3.cloned.1.call-start = ((), (), s32[]{:S(2)}) async-start(), calls=%async_computation.4 | async-start | bytes 655360 | tf_op jit(solution)/shard_map/reduce_scatter | solution.py:79
  (7 other events, 224.7 us)
Sparse Core Ops, SparseCore 0:
  40.2 21.5 all-gather.1
  70.5 31.2 reduce-scatter.4
  179.9 22.0 reduce-scatter.2
where the time goes:
time: 209 us; the launch traced here: 208 us
  starting transfers between devices  67.3 us (32%)
  other arithmetic  40.8 us (20%)
  waiting for transfers between devices  38.1 us (18%)
  blocking collectives  21.7 us (10%)
  matrix products  16.7 us (8%)
  between operations  14 us (7%)
  local copies, waits for them, and re-layouts  8.91 us (4%)
    ppermute x21, starting transfers between devices, passed_along(): return lax.ppermute(array, axis, pairs)  63.7 us
    another operation x8, other arithmetic, block_terms(): suffix = lax.cumsum(keep, axis=3, reverse=True) - keep  35.4 us
    all_to_all x1, blocking collectives, expert_half(): lax.all_to_all(outgoing, 'ep', split_axis=0, concat_axis=0, tiled=True)  21.7 us
    all_gather x1, waiting for transfers between devices, expert_half(): lax.all_gather(lax.all_to_all(outgoing, 'ep', split_axis=0, concat_axis=0...  16.2 us
    reduce_scatter x1, waiting for transfers between devices, attention_half(): lax.psum_scatter(jnp.dot(attended, out_weight, preferred_element_type=jnp...  12.9 us
    all_to_all x1, waiting for transfers between devices, expert_half(): lax.all_to_all(summed, 'ep', split_axis=0, concat_axis=0, tiled=True)  8.86 us
    dot_general x1, matrix products, expert_half(): jnp.einsum('scf,fd->scd', hidden, down_local, preferred_element_type=jnp....  5.02 us
  transfers between devices with their start and end apart: 25, of which 3 were waited for; matrix products, arithmetic and copies ran while one was open for 22% of the time, Pallas kernels for 0%

commit v1 on v0

v1 whole, which is shorter than its diff:
```python
import functools
import math

import jax
import jax.numpy as jnp
from jax import lax
from jax.experimental import pallas as pl
from jax.experimental.pallas import tpu as pltpu
from jax.sharding import PartitionSpec as P

HD = 64
SEQS = 1
GROUPS = 4
F32 = jnp.float32
BF16 = jnp.bfloat16
MESH = pl.DeviceIdType.MESH


def dot(a, b):
    return jnp.dot(a, b, preferred_element_type=F32)


def kernel(
    n, ntp, cap, heads,
    q_ref, k_ref, v_ref, bias_ref, off_ref, wo_hbm, x_ref, gain_ref, idx_ref, rw_ref,
    wg_hbm, wu_hbm, wd_hbm,
    att_out, exp_out,
    kvb, kvs, q4, acc, near, wgu, wd, wo, comb_t, rwt_t, wt, sendx, xs,
    send_a, recv_a, own, send_b, recv_b, res, ret, att_send, att_recv,
    wsem, kv_ss, kv_rs, dx_ss, dx_rs, cr_ss, cr_rs, pa_ss, pa_rs, fw_ss, fw_rs,
    a_ss, a_rs, b_ss, b_rs, r_ss, r_rs, o_ss, o_rs,
):
    me = lax.axis_index("ep")
    tp = lax.axis_index("tp")
    rows = q_ref.shape[0]
    quarter = x_ref.shape[1] // ntp
    ff = wd.shape[0]
    span = n // SEQS
    place = lax.rem(me, span)
    mate = tp + 1 - 2 * lax.rem(tp, 2)
    across = lax.rem(tp + 2, ntp)
    mate_across = lax.rem(mate + 2, ntp)

    barrier = pltpu.get_barrier_semaphore()
    for d in range(1, n):
        pl.semaphore_signal(barrier, inc=1, device_id={"ep": lax.rem(me + d, n)}, device_id_type=MESH)
    for j in range(1, ntp):
        pl.semaphore_signal(barrier, inc=1, device_id={"tp": lax.rem(tp + j, ntp)}, device_id_type=MESH)

    loads = [
        pltpu.make_async_copy(wg_hbm.at[0], wgu.at[:, pl.ds(0, ff)], wsem.at[0]),
        pltpu.make_async_copy(wu_hbm.at[0], wgu.at[:, pl.ds(ff, ff)], wsem.at[1]),
        pltpu.make_async_copy(wd_hbm.at[0], wd, wsem.at[2]),
        pltpu.make_async_copy(wo_hbm, wo, wsem.at[3]),
    ]
    for load in loads:
        load.start()

    def part(d):
        return pl.ds(pl.multiple_of(d * cap, cap), cap)

    def remote(src, dst, ss, rs, where):
        return pltpu.make_async_remote_copy(
            src_ref=src, dst_ref=dst, send_sem=ss, recv_sem=rs, device_id=where, device_id_type=MESH
        )

    def kv_copy(d):
        return remote(kvs, kvb.at[d], kv_ss.at[d], kv_rs.at[d], {"ep": lax.rem(me + d, n)})

    def dx_copy(d):
        return remote(
            sendx.at[part(d)], xs.at[tp, part(d)], dx_ss.at[d], dx_rs.at[d], {"ep": lax.rem(me + d, n)}
        )

    def cross_send(d):
        return remote(xs.at[tp, part(d)], xs.at[tp, part(d)], cr_ss.at[d], cr_rs.at[d], {"tp": across})

    def cross_recv(d):
        return remote(xs.at[across, part(d)], xs.at[across, part(d)], cr_ss.at[d], cr_rs.at[d], {"tp": across})

    def mate_send(d):
        return remote(xs.at[tp, part(d)], xs.at[tp, part(d)], pa_ss.at[d], pa_rs.at[d], {"tp": mate})

    def mate_recv(d):
        return remote(xs.at[mate, part(d)], xs.at[mate, part(d)], pa_ss.at[d], pa_rs.at[d], {"tp": mate})

    def fwd_send(d):
        return remote(xs.at[across, part(d)], xs.at[across, part(d)], fw_ss.at[d], fw_rs.at[d], {"tp": mate})

    def fwd_recv(d):
        return remote(
            xs.at[mate_across, part(d)], xs.at[mate_across, part(d)], fw_ss.at[d], fw_rs.at[d], {"tp": mate}
        )

    kvs[0:rows, :] = jnp.concatenate([k_ref[...], v_ref[...]], axis=1)
    bias_square = jnp.broadcast_to(bias_ref[...].astype(F32), (rows, 128))
    kvs[rows : rows + 16, :] = jnp.transpose(bias_square)[0:16, :].astype(BF16)

    lane = lax.broadcasted_iota(jnp.int32, (rows, 128), 1)
    sub = lax.broadcasted_iota(jnp.int32, (rows, 128), 0)
    first = jnp.where(idx_ref[:, 0:1] == lane, 1.0, 0.0).astype(F32)
    second = jnp.where(idx_ref[:, 1:2] == lane, 1.0, 0.0).astype(F32)
    member = first + second
    below = jnp.where(sub > lane, 1.0, 0.0).astype(F32).astype(BF16)
    slot = dot(below, member.astype(BF16))
    comb_t[...] = jnp.transpose(jnp.where(member > 0.5, slot, -1.0))
    rwt_t[...] = jnp.transpose(first * rw_ref[:, 0:1] + second * rw_ref[:, 1:2])

    x32 = x_ref[...].astype(F32)
    inverse = lax.rsqrt(jnp.mean(x32 * x32, axis=1, keepdims=True) + 1e-06)
    columns = pl.ds(pl.multiple_of(tp * quarter, quarter), quarter)
    normed = (x_ref[:, columns].astype(F32) * inverse * gain_ref[:, columns]).astype(BF16)

    pl.semaphore_wait(barrier, n - 1 + ntp - 1)

    for d in range(1, n):
        @pl.when(place + d < span)
        def _(d=d):
            kv_copy(d).start()

    slot_iota = lax.broadcasted_iota(jnp.int32, (cap, 128), 0).astype(F32)
    for step in range(n):
        d = (step + 1) % n
        e = lax.rem(me + d, n)
        hit = comb_t[pl.ds(e, 1), :] == slot_iota
        wt[d * cap : (d + 1) * cap, :] = jnp.where(hit, rwt_t[pl.ds(e, 1), :], 0.0).astype(BF16)
        picked = dot(jnp.where(hit, 1.0, 0.0).astype(BF16), normed).astype(BF16)
        if d:
            sendx[d * cap : (d + 1) * cap, :] = picked
            dx_copy(d).start()
        else:
            xs[tp, 0:cap, :] = picked
    cross_send(0).start()
    mate_send(0).start()

    strict = jnp.where(sub > lane, 1.0, 0.0).astype(F32).astype(BF16)
    strict2 = jnp.concatenate([strict, strict], axis=0)
    later = sub > lane
    for h in range(heads):
        piece = q_ref[:, h * HD : (h + 1) * HD].astype(F32) * (1.0 / math.sqrt(HD))
        q4[h * rows : (h + 1) * rows, :] = jnp.concatenate(
            [piece, jnp.zeros((rows, 128 - HD), F32)], axis=1
        ).astype(BF16)

    def block(kv_ref, diagonal):
        kv = kv_ref[0:rows, :]
        bias = kv_ref[rows : rows + 16, :].astype(F32)[0:1, :]
        for h in range(heads):
            hs = slice(h * rows, (h + 1) * rows)
            score = lax.dot_general(
                q4[hs, :], kv, (((1,), (1,)), ((), ())), preferred_element_type=F32
            ) + (bias - off_ref[h])
            drop = jnp.maximum(score, 0.0) + jnp.log(1.0 + jnp.exp(-jnp.abs(score)))
            own_log = score - drop
            if diagonal:
                drop = jnp.where(later, drop, 0.0)
            high = drop.astype(BF16)
            low = (drop - high.astype(F32)).astype(BF16)
            after = dot(jnp.concatenate([high, low], axis=1), strict2)
            weight = jnp.exp(own_log - after)
            if diagonal:
                weight = jnp.where(later, weight, 0.0)
            out = dot(weight.astype(BF16), kv)
            total = jnp.broadcast_to(after[:, 0:1] + drop[:, 0:1], (rows, 128))
            if diagonal:
                acc[hs, :] = out
                near[hs, :] = total
            else:
                acc[hs, :] = acc[hs, :] + jnp.exp(-near[hs, :]) * out
                near[hs, :] = near[hs, :] + total

    block(kvs, True)

    def step_of(i, carry):
        dx_copy(i).wait_recv()
        cross_send(i).start()
        mate_send(i).start()
        cross_recv(i - 1).wait_recv()
        fwd_send(i - 1).start()

        @pl.when(place - i >= 0)
        def _():
            kv_copy(i).wait_recv()
            block(kvb.at[i], False)

        return carry

    lax.fori_loop(1, n, step_of, 0)
    cross_recv(n - 1).wait_recv()
    fwd_send(n - 1).start()

    loads[3].wait()
    attended = jnp.concatenate(
        [acc[h * rows : (h + 1) * rows, :][:, HD : 2 * HD] for h in range(heads)], axis=1
    ).astype(BF16)
    att_send[...] = dot(attended, wo[...]).astype(BF16)
    band = rows // ntp

    def att_copy(j):
        peer = lax.rem(tp + j, ntp)
        return remote(
            att_send.at[pl.ds(pl.multiple_of(peer * band, band), band)], att_recv.at[j],
            o_ss.at[j], o_rs.at[j], {"tp": peer},
        )

    for j in range(1, ntp):
        att_copy(j).start()

    for load in loads[0:3]:
        load.wait()
    per = n // GROUPS
    size = per * cap

    def a_copy(g):
        gs = pl.ds(g * size, size)
        return remote(send_a.at[:, gs], recv_a.at[:, gs], a_ss.at[g], a_rs.at[g], {"tp": mate})

    def b_copy(g):
        gs = pl.ds(g * size, size)
        return remote(send_b.at[gs], recv_b.at[gs], b_ss.at[g], b_rs.at[g], {"tp": across})

    def r_copy(d):
        return remote(
            res.at[part(d)], ret.at[part(d)], r_ss.at[d], r_rs.at[d], {"ep": lax.rem(me - d + n, n)}
        )

    def wd_part(q):
        return wd[:, pl.ds(pl.multiple_of(q * quarter, quarter), quarter)]

    for t in range(GROUPS + 2):
        if t < GROUPS:
            gs = slice(t * size, (t + 1) * size)
            for d in range(t * per, (t + 1) * per):
                mate_recv(d).wait_recv()
                fwd_recv(d).wait_recv()
            both = dot(xs[0, gs, :], wgu[0:quarter, :])
            for q in range(1, ntp):
                both = both + dot(xs[q, gs, :], wgu[q * quarter : (q + 1) * quarter, :])
            gate = both[:, 0:ff]
            hidden = (gate / (1.0 + jnp.exp(-gate)) * both[:, ff : 2 * ff]).astype(BF16)
            send_a[0, gs, :] = dot(hidden, wd_part(mate)).astype(BF16)
            send_a[1, gs, :] = dot(hidden, wd_part(mate_across)).astype(BF16)
            a_copy(t).start()
            own[0, gs, :] = dot(hidden, wd_part(tp))
            own[1, gs, :] = dot(hidden, wd_part(across))
        if 1 <= t <= GROUPS:
            g = t - 1
            gs = slice(g * size, (g + 1) * size)
            a_copy(g).wait_recv()
            send_b[gs, :] = (own[1, gs, :] + recv_a[1, gs, :].astype(F32)).astype(BF16)
            b_copy(g).start()
        if t >= 2:
            g = t - 2
            gs = slice(g * size, (g + 1) * size)
            b_copy(g).wait_recv()
            final = (
                own[0, gs, :] + recv_a[0, gs, :].astype(F32) + recv_b[gs, :].astype(F32)
            ).astype(BF16)
            res[gs, :] = final
            for d in range(g * per, (g + 1) * per):
                if d:
                    r_copy(d).start()
            if g == 0:
                ret[0:cap, :] = final[0:cap, :]

    for j in range(1, ntp):
        att_copy(j).wait_recv()
    summed = att_send[pl.ds(pl.multiple_of(tp * band, band), band), :].astype(F32)
    for j in range(1, ntp):
        summed = summed + att_recv[j].astype(F32)
    att_out[...] = summed.astype(BF16)

    for d in range(1, n):
        r_copy(d).wait_recv()
    exp_out[...] = lax.dot_general(
        wt[...], ret[...], (((0,), (0,)), ((), ())), preferred_element_type=F32
    ).astype(BF16)

    for d in range(1, n):
        @pl.when(place + d < span)
        def _(d=d):
            kv_copy(d).wait_send()

        dx_copy(d).wait_send()
        r_copy(d).wait_send()
    for d in range(n):
        cross_send(d).wait_send()
        mate_send(d).wait_send()
        fwd_send(d).wait_send()
    for g in range(GROUPS):
        a_copy(g).wait_send()
        b_copy(g).wait_send()
    for j in range(1, ntp):
        att_copy(j).wait_send()


def body(n, ntp, q, k, v, bias, off, wo, x, gain, idx, rw, wg, wu, wd):
    rows, tokens, width = q.shape[0], x.shape[0], x.shape[1]
    heads = q.shape[1] // HD
    cap = max(16, -(-2 * tokens * idx.shape[1] // n // 16) * 16)
    total = n * cap
    quarter = width // ntp
    ff = wd.shape[1]
    band = rows // ntp
    vmem = pl.BlockSpec(memory_space=pltpu.VMEM)
    anyspace = pl.BlockSpec(memory_space=pl.ANY)
    smem = pl.BlockSpec(memory_space=pltpu.SMEM)
    dma = pltpu.SemaphoreType.DMA
    return pl.pallas_call(
        functools.partial(kernel, n, ntp, cap, heads),
        out_shape=(
            jax.ShapeDtypeStruct((band, wo.shape[1]), BF16),
            jax.ShapeDtypeStruct((tokens, quarter), BF16),
        ),
        in_specs=[vmem, vmem, vmem, vmem, smem, anyspace, vmem, vmem, vmem, vmem, anyspace, anyspace, anyspace],
        out_specs=(vmem, vmem),
        scratch_shapes=[
            pltpu.VMEM((n, rows + 16, 128), BF16),
            pltpu.VMEM((rows + 16, 128), BF16),
            pltpu.VMEM((heads * rows, 128), BF16),
            pltpu.VMEM((heads * rows, 128), F32),
            pltpu.VMEM((heads * rows, 128), F32),
            pltpu.VMEM((width, 2 * ff), BF16),
            pltpu.VMEM((ff, width), BF16),
            pltpu.VMEM(wo.shape, BF16),
            pltpu.VMEM((128, tokens), F32),
            pltpu.VMEM((128, tokens), F32),
            pltpu.VMEM((total, tokens), BF16),
            pltpu.VMEM((total, quarter), BF16),
            pltpu.VMEM((ntp, total, quarter), BF16),
            pltpu.VMEM((2, total, quarter), BF16),
            pltpu.VMEM((2, total, quarter), BF16),
            pltpu.VMEM((2, total, quarter), F32),
            pltpu.VMEM((total, quarter), BF16),
            pltpu.VMEM((total, quarter), BF16),
            pltpu.VMEM((total, quarter), BF16),
            pltpu.VMEM((total, quarter), BF16),
            pltpu.VMEM((rows, wo.shape[1]), BF16),
            pltpu.VMEM((ntp, band, wo.shape[1]), BF16),
            dma((4,)),
        ]
        + [dma((n,))] * 10
        + [dma((GROUPS,))] * 4
        + [dma((n,))] * 2
        + [dma((ntp,))] * 2,
        compiler_params=pltpu.CompilerParams(collective_id=0, has_side_effects=True),
    )(q, k, v, bias, off, wo, x, gain.reshape(1, -1), idx, rw, wg, wu, wd)


def solution(mesh):
    return jax.shard_map(
        functools.partial(body, mesh.shape["ep"], mesh.shape["tp"]),
        mesh=mesh,
        in_specs=(
            P("ep", "tp"),
            P("ep", "tp"),
            P("ep", "tp"),
            P("ep", "tp"),
            P("tp"),
            P("tp", None),
            P("ep", None),
            P(),
            P("ep", None),
            P("ep", None),
            P("ep", None, "tp"),
            P("ep", None, "tp"),
            P("ep", "tp", None),
        ),
        out_specs=(P(("ep", "tp"), None), P("ep", "tp")),
        check_vma=False,
    )
```

time: 209 us -> 72.2 us (0.35)
  starting transfers between devices: 67.3 us -> 0 us
  Pallas kernels: 0 us -> 64.6 us
  other arithmetic: 40.8 us -> 0 us
  waiting for transfers between devices: 38.1 us -> 0 us
  blocking collectives: 21.7 us -> 0 us
  matrix products: 16.7 us -> 0 us
  between operations: 14 us -> 0.66 us
  local copies, waits for them, and re-layouts: 8.91 us -> 6.62 us
    pallas_call x0 -> x1, Pallas kernels: none -> 64.6 us  [body(): pl.pallas_call(functools.partial(kernel, n, ntp, cap, heads), out_shape=(...]
    ppermute x21 -> x0, starting transfers between devices: 63.7 us -> none  [passed_along(): return lax.ppermute(array, axis, pairs)]
    another operation x10 -> x0, other arithmetic: 36 us -> none  [the longest x8 35.4 us: block_terms(): suffix = lax.cumsum(keep, axis=3, reverse=True) - keep]
    all_to_all x1 -> x0, blocking collectives: 21.7 us -> none  [expert_half(): lax.all_to_all(outgoing, 'ep', split_axis=0, concat_axis=0, tiled=True)]
    dot_general x19 -> x0, matrix products: 16.7 us -> none  [the longest x1 5.02 us: expert_half(): jnp.einsum('scf,fd->scd', hidden, down_local, preferred_element_type=jnp....]
    all_gather x1 -> x0, waiting for transfers between devices: 16.2 us -> none  [expert_half(): lax.all_gather(lax.all_to_all(outgoing, 'ep', split_axis=0, concat_axis=0...]
    reduce_scatter x2 -> x0, waiting for transfers between devices: 12.9 us -> none  [the longest x1 12.9 us: attention_half(): lax.psum_scatter(jnp.dot(attended, out_weight, preferred_element_type=jnp...]
    all_to_all x1 -> x0, waiting for transfers between devices: 8.86 us -> none  [expert_half(): lax.all_to_all(summed, 'ep', split_axis=0, concat_axis=0, tiled=True)]
  transfers between devices with their start and end apart: 25 -> 0, of which waited for: 3 -> 0; matrix products, arithmetic and copies ran while one was open for 22% -> 0% of each run, Pallas kernels for 0% -> 0%
where the time goes in v1:
time: 72.2 us; the launch traced here: 71.9 us
  Pallas kernels  64.6 us (89%)
  local copies, waits for them, and re-layouts  6.62 us (9%)
    pallas_call x1, Pallas kernels, body(): pl.pallas_call(functools.partial(kernel, n, ntp, cap, heads), out_shape=(...  64.6 us
    unnamed x17, local copies, waits for them, and re-layouts  6.62 us

profile of v1, /device:TPU:0, one launch (start us, length us, event | category | flops | bytes accessed | tf_op | source)
XLA Modules:
  0.0 71.9 jit_solution(1735526733454613283)
XLA Ops:
  0.6 0.0 copy-start.1
  0.6 1.4 %copy.15.k_ref = bf16[128,64]{1,0:T(8,128)(2,1)} copy(bf16[128,64]{0,1:T(8,128)(2,1)} %param.14) | data formatting | bytes 32768 | tf_op args[1]
  2.1 0.0 copy-done.1
  2.1 0.0 copy-start.4
  2.1 0.7 copy.16.v_ref
  2.8 0.0 copy-done.4
  2.8 0.0 copy-start.2
  2.8 0.7 %copy.17.bias_ref = bf16[128,1]{1,0:T(8,128)(2,1)} copy(bf16[128,1]{0,1:T(2,128)(2,1)S(1)} %copy-done.4) | data formatting | bytes 512 | tf_op args[3]
  3.5 0.0 copy-done.2
  3.5 0.0 copy-start.3
  3.5 0.7 %copy.18.idx_ref = s32[128,2]{1,0:T(8,128)} copy(s32[128,2]{0,1:T(2,128)S(1)} %copy-done.2) | data formatting | bytes 2048 | tf_op args[8]
  4.3 0.0 copy-done.3
  4.3 0.7 %copy.19.rw_ref = f32[128,2]{1,0:T(8,128)} copy(f32[128,2]{0,1:T(2,128)S(1)} %copy-done.3) | data formatting | bytes 2048 | tf_op args[9]
  5.0 64.6 %shard_map.140 = (bf16[32,2048]{1,0:T(8,128)(2,1)}, bf16[128,512]{1,0:T(8,128)(2,1)}) custom-call(bf16[128,256]{1,0:T(8,128)(2,1)} %q_ref.1, bf16[128,64]{1,0:T(8,128)(2,1)} %copy.15.k_ref, bf16[128,64]{1,0:T(8,128)(2,1)} %copy.16.v_ref, bf16[128,1]{1,0:T(8,128)(2,1)} %copy.17.bias_ref, f32[4]{0:T(128)} %off_ref.1, bf16[256,2048]{1,0:T(8,128)(2,1)} %wo_hbm.1, ...), custom_call_target="tpu_custom_call" | custom-call | tf_op jit(solution)/shard_map/pallas_call | solution.py:309
  69.6 0.0 copy-start
  69.7 1.6 %copy.22 = bf16[32,2048]{1,0:T(8,128)(2,1)} copy(bf16[32,2048]{1,0:T(8,128)(2,1)} %get-tuple-element.4) | data formatting | bytes 262144
  71.3 0.0 copy-done
  71.3 0.7 copy.23
Async XLA Ops:
  0.6 1.4 %copy-start.1 = (bf16[128,64]{0,1:T(8,128)(2,1)S(1)}, bf16[128,64]{0,1:T(8,128)(2,1)}, u32[]{:S(2)}) copy-start(bf16[128,64]{0,1:T(8,128)(2,1)} %param.15) | copy-start | bytes 49156
  2.1 0.7 copy-start.4
  2.8 0.7 %copy-start.2 = (s32[128,2]{0,1:T(2,128)S(1)}, s32[128,2]{0,1:T(2,128)}, u32[]{:S(2)}) copy-start(s32[128,2]{0,1:T(2,128)} %param.21) | copy-start | bytes 3076
  3.5 0.7 %copy-start.3 = (f32[128,2]{0,1:T(2,128)S(1)}, f32[128,2]{0,1:T(2,128)}, u32[]{:S(2)}) copy-start(f32[128,2]{0,1:T(2,128)} %param.22) | copy-start | bytes 3076
  69.6 1.6 %copy-start = (bf16[128,512]{1,0:T(8,128)(2,1)S(1)}, bf16[128,512]{1,0:T(8,128)(2,1)}, u32[]{:S(2)}) copy-start(bf16[128,512]{1,0:T(8,128)(2,1)} %get-tuple-element.5) | copy-start | bytes 393220

commit v2 on v1

--- a/solution.py
+++ b/solution.py
@@ -92,19 +92,19 @@
             xs.at[mate_across, part(d)], xs.at[mate_across, part(d)], fw_ss.at[d], fw_rs.at[d], {"tp": mate}
         )
 
-    kvs[0:rows, :] = jnp.concatenate([k_ref[...], v_ref[...]], axis=1)
-    bias_square = jnp.broadcast_to(bias_ref[...].astype(F32), (rows, 128))
-    kvs[rows : rows + 16, :] = jnp.transpose(bias_square)[0:16, :].astype(BF16)
-
-    lane = lax.broadcasted_iota(jnp.int32, (rows, 128), 1)
-    sub = lax.broadcasted_iota(jnp.int32, (rows, 128), 0)
-    first = jnp.where(idx_ref[:, 0:1] == lane, 1.0, 0.0).astype(F32)
-    second = jnp.where(idx_ref[:, 1:2] == lane, 1.0, 0.0).astype(F32)
+    kvs[0:HD, :] = k_ref[...]
+    kvs[HD : 2 * HD, :] = v_ref[...]
+    kvs[2 * HD : 2 * HD + 16, :] = jnp.broadcast_to(bias_ref[...].astype(F32), (16, rows)).astype(BF16)
+
+    lane = lax.broadcasted_iota(jnp.int32, (128, rows), 1)
+    sub = lax.broadcasted_iota(jnp.int32, (128, rows), 0)
+    first = jnp.where(idx_ref[0:1, :] == sub, 1.0, 0.0).astype(F32)
+    second = jnp.where(idx_ref[1:2, :] == sub, 1.0, 0.0).astype(F32)
     member = first + second
-    below = jnp.where(sub > lane, 1.0, 0.0).astype(F32).astype(BF16)
-    slot = dot(below, member.astype(BF16))
-    comb_t[...] = jnp.transpose(jnp.where(member > 0.5, slot, -1.0))
-    rwt_t[...] = jnp.transpose(first * rw_ref[:, 0:1] + second * rw_ref[:, 1:2])
+    above = jnp.where(sub < lane, 1.0, 0.0).astype(F32).astype(BF16)
+    slot = dot(member.astype(BF16), above)
+    comb_t[...] = jnp.where(member > 0.5, slot, -1.0)
+    rwt_t[...] = first * rw_ref[0:1, :] + second * rw_ref[1:2, :]
 
     x32 = x_ref[...].astype(F32)
     inverse = lax.rsqrt(jnp.mean(x32 * x32, axis=1, keepdims=True) + 1e-06)
@@ -113,14 +113,9 @@
 
     pl.semaphore_wait(barrier, n - 1 + ntp - 1)
 
-    for d in range(1, n):
-        @pl.when(place + d < span)
-        def _(d=d):
-            kv_copy(d).start()
-
     slot_iota = lax.broadcasted_iota(jnp.int32, (cap, 128), 0).astype(F32)
     for step in range(n):
-        d = (step + 1) % n
+        d = step
         e = lax.rem(me + d, n)
         hit = comb_t[pl.ds(e, 1), :] == slot_iota
         wt[d * cap : (d + 1) * cap, :] = jnp.where(hit, rwt_t[pl.ds(e, 1), :], 0.0).astype(BF16)
@@ -130,8 +125,13 @@
             dx_copy(d).start()
         else:
             xs[tp, 0:cap, :] = picked
-    cross_send(0).start()
-    mate_send(0).start()
+            cross_send(0).start()
+            mate_send(0).start()
+    for d in range(1, n):
+        @pl.when(place + d < span)
+        def _(d=d):
+            kv_copy(d).start()
+
 
     strict = jnp.where(sub > lane, 1.0, 0.0).astype(F32).astype(BF16)
     strict2 = jnp.concatenate([strict, strict], axis=0)
@@ -143,13 +143,11 @@
         ).astype(BF16)
 
     def block(kv_ref, diagonal):
-        kv = kv_ref[0:rows, :]
-        bias = kv_ref[rows : rows + 16, :].astype(F32)[0:1, :]
+        kv = kv_ref[0 : 2 * HD, :]
+        bias = kv_ref[2 * HD : 2 * HD + 16, :].astype(F32)[0:1, :]
         for h in range(heads):
             hs = slice(h * rows, (h + 1) * rows)
-            score = lax.dot_general(
-                q4[hs, :], kv, (((1,), (1,)), ((), ())), preferred_element_type=F32
-            ) + (bias - off_ref[h])
+            score = dot(q4[hs, :], kv) + (bias - off_ref[h])
             drop = jnp.maximum(score, 0.0) + jnp.log(1.0 + jnp.exp(-jnp.abs(score)))
             own_log = score - drop
             if diagonal:
@@ -160,7 +158,9 @@
             weight = jnp.exp(own_log - after)
             if diagonal:
                 weight = jnp.where(later, weight, 0.0)
-            out = dot(weight.astype(BF16), kv)
+            out = lax.dot_general(
+                weight.astype(BF16), kv, (((1,), (1,)), ((), ())), preferred_element_type=F32
+            )
             total = jnp.broadcast_to(after[:, 0:1] + drop[:, 0:1], (rows, 128))
             if diagonal:
                 acc[hs, :] = out
@@ -172,12 +172,6 @@
     block(kvs, True)
 
     def step_of(i, carry):
-        dx_copy(i).wait_recv()
-        cross_send(i).start()
-        mate_send(i).start()
-        cross_recv(i - 1).wait_recv()
-        fwd_send(i - 1).start()
-
         @pl.when(place - i >= 0)
         def _():
             kv_copy(i).wait_recv()
@@ -185,83 +179,101 @@
 
         return carry
 
+    band = rows // ntp
+
+    def att_copy(j):
+        peer = lax.rem(tp + j, ntp)
+        return remote(
+            att_send.at[pl.ds(pl.multiple_of(peer * band, band), band)], att_recv.at[j],
+            o_ss.at[j], o_rs.at[j], {"tp": peer},
+        )
+
+    for load in loads[0:3]:
+        load.wait()
+    per = n // GROUPS
+    size = per * cap
+
+    def a_copy(g):
+        gs = pl.ds(g * size, size)
+        return remote(send_a.at[:, gs], recv_a.at[:, gs], a_ss.at[g], a_rs.at[g], {"tp": mate})
+
+    def b_copy(g):
+        gs = pl.ds(g * size, size)
+        return remote(send_b.at[gs], recv_b.at[gs], b_ss.at[g], b_rs.at[g], {"tp": across})
+
+    def r_copy(d):
+        return remote(
+            res.at[part(d)], ret.at[part(d)], r_ss.at[d], r_rs.at[d], {"ep": lax.rem(me - d + n, n)}
+        )
+
+    def wd_part(q):
+        return wd[:, pl.ds(pl.multiple_of(q * quarter, quarter), quarter)]
+
+    def collect(g):
+        for d in range(max(1, g * per), (g + 1) * per):
+            dx_copy(d).wait_recv()
+            cross_send(d).start()
+            mate_send(d).start()
+
+    def forward(g):
+        for d in range(g * per, (g + 1) * per):
+            cross_recv(d).wait_recv()
+            fwd_send(d).start()
+
+    def expert(g):
+        gs = slice(g * size, (g + 1) * size)
+        for d in range(g * per, (g + 1) * per):
+            mate_recv(d).wait_recv()
+            fwd_recv(d).wait_recv()
+        both = dot(xs[0, gs, :], wgu[0:quarter, :])
+        for q in range(1, ntp):
+            both = both + dot(xs[q, gs, :], wgu[q * quarter : (q + 1) * quarter, :])
+        gate = both[:, 0:ff]
+        hidden = (gate / (1.0 + jnp.exp(-gate)) * both[:, ff : 2 * ff]).astype(BF16)
+        send_a[1, gs, :] = dot(hidden, wd_part(mate_across)).astype(BF16)
+        send_a[0, gs, :] = dot(hidden, wd_part(mate)).astype(BF16)
+        a_copy(g).start()
+        own[1, gs, :] = dot(hidden, wd_part(across))
+        own[0, gs, :] = dot(hidden, wd_part(tp))
+
+    def reduce_near(g):
+        gs = slice(g * size, (g + 1) * size)
+        a_copy(g).wait_recv()
+        send_b[gs, :] = (own[1, gs, :] + recv_a[1, gs, :].astype(F32)).astype(BF16)
+        b_copy(g).start()
+
+    def give_back(g):
+        gs = slice(g * size, (g + 1) * size)
+        b_copy(g).wait_recv()
+        final = (own[0, gs, :] + recv_a[0, gs, :].astype(F32) + recv_b[gs, :].astype(F32)).astype(BF16)
+        res[gs, :] = final
+        for d in range(max(1, g * per), (g + 1) * per):
+            r_copy(d).start()
+        if g == 0:
+            ret[0:cap, :] = final[0:cap, :]
+
+    for t in range(GROUPS + 2):
+        if t < GROUPS:
+            collect(t)
+        if 1 <= t <= GROUPS:
+            forward(t - 1)
+        if 2 <= t:
+            reduce_near(t - 2)
+        if 3 <= t:
+            give_back(t - 3)
+        if 1 <= t <= GROUPS:
+            expert(t - 1)
+
     lax.fori_loop(1, n, step_of, 0)
-    cross_recv(n - 1).wait_recv()
-    fwd_send(n - 1).start()
-
     loads[3].wait()
     attended = jnp.concatenate(
         [acc[h * rows : (h + 1) * rows, :][:, HD : 2 * HD] for h in range(heads)], axis=1
     ).astype(BF16)
     att_send[...] = dot(attended, wo[...]).astype(BF16)
-    band = rows // ntp
-
-    def att_copy(j):
-        peer = lax.rem(tp + j, ntp)
-        return remote(
-            att_send.at[pl.ds(pl.multiple_of(peer * band, band), band)], att_recv.at[j],
-            o_ss.at[j], o_rs.at[j], {"tp": peer},
-        )
-
     for j in range(1, ntp):
         att_copy(j).start()
 
-    for load in loads[0:3]:
-        load.wait()
-    per = n // GROUPS
-    size = per * cap
-
-    def a_copy(g):
-        gs = pl.ds(g * size, size)
-        return remote(send_a.at[:, gs], recv_a.at[:, gs], a_ss.at[g], a_rs.at[g], {"tp": mate})
-
-    def b_copy(g):
-        gs = pl.ds(g * size, size)
-        return remote(send_b.at[gs], recv_b.at[gs], b_ss.at[g], b_rs.at[g], {"tp": across})
-
-    def r_copy(d):
-        return remote(
-            res.at[part(d)], ret.at[part(d)], r_ss.at[d], r_rs.at[d], {"ep": lax.rem(me - d + n, n)}
-        )
-
-    def wd_part(q):
-        return wd[:, pl.ds(pl.multiple_of(q * quarter, quarter), quarter)]
-
-    for t in range(GROUPS + 2):
-        if t < GROUPS:
-            gs = slice(t * size, (t + 1) * size)
-            for d in range(t * per, (t + 1) * per):
-                mate_recv(d).wait_recv()
-                fwd_recv(d).wait_recv()
-            both = dot(xs[0, gs, :], wgu[0:quarter, :])
-            for q in range(1, ntp):
-                both = both + dot(xs[q, gs, :], wgu[q * quarter : (q + 1) * quarter, :])
-            gate = both[:, 0:ff]
-            hidden = (gate / (1.0 + jnp.exp(-gate)) * both[:, ff : 2 * ff]).astype(BF16)
-            send_a[0, gs, :] = dot(hidden, wd_part(mate)).astype(BF16)
-            send_a[1, gs, :] = dot(hidden, wd_part(mate_across)).astype(BF16)
-            a_copy(t).start()
-            own[0, gs, :] = dot(hidden, wd_part(tp))
-            own[1, gs, :] = dot(hidden, wd_part(across))
-        if 1 <= t <= GROUPS:
-            g = t - 1
-            gs = slice(g * size, (g + 1) * size)
-            a_copy(g).wait_recv()
-            send_b[gs, :] = (own[1, gs, :] + recv_a[1, gs, :].astype(F32)).astype(BF16)
-            b_copy(g).start()
-        if t >= 2:
-            g = t - 2
-            gs = slice(g * size, (g + 1) * size)
-            b_copy(g).wait_recv()
-            final = (
-                own[0, gs, :] + recv_a[0, gs, :].astype(F32) + recv_b[gs, :].astype(F32)
-            ).astype(BF16)
-            res[gs, :] = final
-            for d in range(g * per, (g + 1) * per):
-                if d:
-                    r_copy(d).start()
-            if g == 0:
-                ret[0:cap, :] = final[0:cap, :]
+    give_back(GROUPS - 1)
 
     for j in range(1, ntp):
         att_copy(j).wait_recv()
@@ -315,8 +327,8 @@
         in_specs=[vmem, vmem, vmem, vmem, smem, anyspace, vmem, vmem, vmem, vmem, anyspace, anyspace, anyspace],
         out_specs=(vmem, vmem),
         scratch_shapes=[
-            pltpu.VMEM((n, rows + 16, 128), BF16),
-            pltpu.VMEM((rows + 16, 128), BF16),
+            pltpu.VMEM((n, 2 * HD + 16, rows), BF16),
+            pltpu.VMEM((2 * HD + 16, rows), BF16),
             pltpu.VMEM((heads * rows, 128), BF16),
             pltpu.VMEM((heads * rows, 128), F32),
             pltpu.VMEM((heads * rows, 128), F32),
@@ -344,7 +356,7 @@
         + [dma((n,))] * 2
         + [dma((ntp,))] * 2,
         compiler_params=pltpu.CompilerParams(collective_id=0, has_side_effects=True),
-    )(q, k, v, bias, off, wo, x, gain.reshape(1, -1), idx, rw, wg, wu, wd)
+    )(q, k.T, v.T, bias.T, off, wo, x, gain.reshape(1, -1), idx.T, rw.T, wg, wu, wd)
 
 
 def solution(mesh):

time: 72.2 us -> 56.9 us (0.79)
  Pallas kernels: 64.6 us -> 53.9 us
  local copies, waits for them, and re-layouts: 6.62 us -> 2.26 us
    pallas_call x1, Pallas kernels: 64.6 us -> 53.9 us  [body(): pl.pallas_call(functools.partial(kernel, n, ntp, cap, heads), out_shape=(...]
    unnamed x17 -> x4, local copies, waits for them, and re-layouts: 6.62 us -> 2.26 us
where the time goes in v2:
time: 56.9 us; the launch traced here: 56.8 us
  Pallas kernels  53.9 us (95%)
  local copies, waits for them, and re-layouts  2.26 us (4%)
  between operations  0.65 us (1%)
    pallas_call x1, Pallas kernels, body(): pl.pallas_call(functools.partial(kernel, n, ntp, cap, heads), out_shape=(...  53.9 us
    unnamed x4, local copies, waits for them, and re-layouts  2.26 us

profile of v2, /device:TPU:0, one launch (start us, length us, event | category | flops | bytes accessed | tf_op | source)
XLA Modules:
  0.0 56.8 jit_solution(12140722605434029508)
XLA Ops:
  0.6 53.9 %shard_map.140 = (bf16[32,2048]{1,0:T(8,128)(2,1)}, bf16[128,512]{1,0:T(8,128)(2,1)}) custom-call(bf16[128,256]{1,0:T(8,128)(2,1)} %q_ref.1, bf16[64,128]{1,0:T(8,128)(2,1)} %bitcast.6, bf16[64,128]{1,0:T(8,128)(2,1)} %bitcast.7, bf16[1,128]{1,0:T(2,128)(2,1)} %bitcast.11, f32[4]{0:T(128)} %off_ref.1, bf16[256,2048]{1,0:T(8,128)(2,1)} %wo_hbm.1, ...), custom_call_target="tpu_custom_call" | custom-call | tf_op jit(solution)/shard_map/pallas_call | solution.py:321
  54.5 0.0 copy-start
  54.5 1.6 %copy.17 = bf16[32,2048]{1,0:T(8,128)(2,1)} copy(bf16[32,2048]{1,0:T(8,128)(2,1)} %get-tuple-element.4) | data formatting | bytes 262144
  56.1 0.0 copy-done
  56.1 0.7 %copy.18 = bf16[128,512]{1,0:T(8,128)(2,1)} copy(bf16[128,512]{1,0:T(8,128)(2,1)S(1)} %copy-done) | data formatting | bytes 262144
Async XLA Ops:
  54.5 1.6 %copy-start = (bf16[128,512]{1,0:T(8,128)(2,1)S(1)}, bf16[128,512]{1,0:T(8,128)(2,1)}, u32[]{:S(2)}) copy-start(bf16[128,512]{1,0:T(8,128)(2,1)} %get-tuple-element.5) | copy-start | bytes 393220
